TPU v7x, 256 devices: a whole 4x4x8 slice. The times are simulated.
256 devices in a mesh: ra: 32 (over z, y), cb: 4 (over x), dp: 2 (over core).
Axes of the slice: x: 4, y: 4, z: 8, core: 2. Of those that a mesh axis runs over, the one named last changes fastest.
Arguments:
- stream: bfloat16 [3072, 4096], P(('cb', 'dp'), 'ra'), may hold values from -20 to 20
- up_first: bfloat16 [4096, 16384], P('cb', 'ra'), may hold values from -0.09375 to 0.09375
- down_first: bfloat16 [16384, 4096], P('ra', 'cb'), may hold values from -0.046875 to 0.046875
- up_second: bfloat16 [4096, 16384], P('cb', 'ra'), may hold values from -0.09375 to 0.09375
- down_second: bfloat16 [16384, 4096], P('ra', 'cb'), may hold values from -0.046875 to 0.046875
- gain_first: float32 [4096], P('ra'), may hold values from 0.1 to 1.9
- bias_first: float32 [4096], P('ra'), may hold values from -3 to 3
- gain_second: float32 [4096], P('ra'), may hold values from 0.1 to 1.9
- bias_second: float32 [4096], P('ra'), may hold values from -3 to 3
Outputs:
- result: bfloat16 [3072, 4096], P(('cb', 'dp'), 'ra')
All inputs are finite; a program needn't handle non-finite values.
Results may differ from a plain program's by a relative error of at most 0.0093.
Values may be sent and summed in bfloat16 or wider, within the bound.
No kernel may reach another device: no remote copies, remote signals or barrier semaphores. Data moves between devices by JAX's collectives and lax.ppermute only.
A program may use at most 64 MiB of HBM per device.

v0:
```python
import jax
import jax.numpy as jnp
from jax import lax
from jax.sharding import Mesh
from jax.sharding import PartitionSpec as P

RA = ("ra_0", "ra_1")
RESID = 1.4142135
EPS = 0.5


def whole_of(shard, axes, dim):
    for axis in reversed(axes):
        shard = lax.all_gather(shard, axis, axis=dim, tiled=True)
    return shard


def cut_along(shard, dim, length):
    lengths = shard.shape
    blocks = shard.reshape(*lengths[:dim], length, lengths[dim] // length, *lengths[dim + 1 :])
    return jnp.moveaxis(blocks, dim, 0)


def summed_on_arrival(shard, axis, dim):
    length = lax.axis_size(axis)
    blocks = lax.all_to_all(cut_along(shard, dim, length), axis, 0, 0, tiled=True)
    return jnp.sum(blocks.astype(jnp.float32), axis=0)


def copy_for_each(shard, axis):
    length = lax.axis_size(axis)
    return lax.all_to_all(
        jnp.broadcast_to(shard[None], (length, *shard.shape)), axis, 0, 0, tiled=True
    )


def over_copies(shard, axis):
    everything = copy_for_each(shard, axis)
    return jnp.sum(everything, axis=0)


def in_one(arrays, axis):
    ravelled, at, done = (jnp.concatenate([a.reshape(-1) for a in arrays]), 0, [])
    subtotal = over_copies(ravelled, axis)
    for a in arrays:
        done.append(subtotal[at : at + a.size].reshape(a.shape))
        at += a.size
    return tuple(done)


def sublayer(x, up, down, gain, bias):
    whole = whole_of(x, RA, 1)
    pre = jnp.dot(
        whole, lax.all_gather(up, "cb", axis=0, tiled=True), preferred_element_type=jnp.float32
    )
    hidden = jnp.square(jax.nn.relu(pre)).astype(jnp.bfloat16)
    partial_sums = jnp.dot(
        hidden, lax.all_gather(down, "cb", axis=1, tiled=True), preferred_element_type=jnp.float32
    )
    branch = summed_on_arrival(partial_sums.astype(jnp.bfloat16), RA, 1)
    mixed = RESID * x.astype(jnp.float32) + branch
    width = mixed.shape[1] * lax.axis_size(RA)
    total, squares = in_one(
        (jnp.sum(mixed, axis=1, keepdims=True), jnp.sum(mixed * mixed, axis=1, keepdims=True)), RA
    )
    mean = total / width
    var = squares / width - mean * mean
    centered = mixed - mean
    return (centered * lax.rsqrt(var + EPS) * gain + bias).astype(jnp.bfloat16)


def body(
    stream,
    up_first,
    down_first,
    up_second,
    down_second,
    gain_first,
    bias_first,
    gain_second,
    bias_second,
):
    x = stream
    for up, down, gain, bias in (
        (up_first, down_first, gain_first, bias_first),
        (up_second, down_second, gain_second, bias_second),
    ):
        x = sublayer(x, up, down, gain, bias)
    return x


def solution(mesh):
    torus = Mesh(
        mesh.devices.reshape(8, 4, mesh.shape["cb"], mesh.shape["dp"]), ("ra_0", "ra_1", "cb", "dp")
    )
    in_specs = (
        P(("cb", "dp"), RA),
        P("cb", RA),
        P(RA, "cb"),
        P("cb", RA),
        P(RA, "cb"),
        P(RA),
        P(RA),
        P(RA),
        P(RA),
    )
    out_specs = P(("cb", "dp"), RA)
    return jax.shard_map(body, mesh=torus, in_specs=in_specs, out_specs=out_specs, check_vma=False)
```

profile of v0, /device:TPU:2, one launch (start us, length us, event | category | flops | bytes accessed | tf_op | source)
XLA Modules:
  0.0 448.1 jit_solution(4265126801284976559)
XLA Ops:
  6.5 0.0 all-gather.7.cloned.1.call-start
  6.5 13.8 %all_gather.24 = bf16[384,512]{1,0:T(8,128)(2,1)} all-gather(bf16[384,128]{1,0:T(8,128)(2,1)} %param.9), channel_id=1, replica_groups=mesh['ra_0'=8,'ra_1'=4,'cb'=4,'dp'=2] {'ra_1'}, dimensions={1}, use_global_device_ids=true | all-gather | bytes 491520 | tf_op jit(solution)/shard_map/all_gather | solution.py:14
  20.4 0.0 all-gather.7.cloned.1.call-update
  20.4 0.0 all-gather.11.cloned.1.call-start
  20.5 0.7 all-gather.11.cloned.1.call-update
  21.2 0.0 all-gather.9.cloned.1.call-start
  21.2 0.7 all-gather.9.cloned.1.call-update
  21.9 0.0 all-gather.15.cloned.1.call-start
  21.9 0.5 all-gather.15.cloned.1.call-update
  22.5 46.4 %all-gather.7.cloned.1.call-done = bf16[384,4096]{1,0:T(8,128)(2,1)} async-done(((bf16[384,512]{1,0:T(8,128)(2,1)}), bf16[384,4096]{1,0:T(8,128)(2,1)}) %all-gather.7.cloned.1.call-update) | async-done | bytes 3145744 | tf_op jit(solution)/shard_map/all_gather | solution.py:14
  68.9 50.6 %all-gather.11.cloned.1.call-done = bf16[512,4096]{1,0:T(8,128)(2,1)} async-done(((bf16[512,1024]{1,0:T(8,128)(2,1)}), bf16[512,4096]{1,0:T(8,128)(2,1)}) %all-gather.11.cloned.1.call-update) | async-done | bytes 4194320 | tf_op jit(solution)/shard_map/all_gather | solution.py:58
  119.4 53.0 %all-gather.9.cloned.1.call-done = bf16[4096,512]{1,0:T(8,128)(2,1)} async-done(((bf16[1024,512]{1,0:T(8,128)(2,1)}), bf16[4096,512]{1,0:T(8,128)(2,1)}) %all-gather.9.cloned.1.call-update) | async-done | bytes 4194320 | tf_op jit(solution)/shard_map/all_gather | solution.py:54
  172.4 7.8 %fusion = bf16[48,32,8,128]{3,2,1,0:T(8,128)(2,1)S(1)} fusion(bf16[512,4096]{1,0:T(8,128)(2,1)} %all-gather.11.cloned.1.call-done, bf16[384,4096]{1,0:T(8,128)(2,1)} %all-gather.7.cloned.1.call-done, bf16[4096,512]{1,0:T(8,128)(2,1)} %all-gather.9.cloned.1.call-done), kind=kOutput, calls=%fused_computation.6 | convolution fusion | flops 3223388160 | bytes 14680064 | tf_op jit(solution)/shard_map/dot_general | solution.py:57
  180.2 2.6 copy.29
  182.8 0.0 copy-start
  182.8 0.0 copy-start.1
  182.8 0.0 copy-start.2
  182.8 10.0 %all-to-all-start = ((bf16[32,384,128]{2,1,0:T(8,128)(2,1)}), bf16[32,384,128]{2,1,0:T(8,128)(2,1)S(1)}, u32[]{:S(2)}, u32[]{:S(2)}) async-start(bf16[32,384,128]{2,1,0:T(8,128)(2,1)} %bitcast.22), calls=%async_computation | async-start | bytes 6291456 | tf_op jit(solution)/shard_map/all_to_all | solution.py:26
  192.8 0.0 all-gather.17.cloned.1.call-start
  192.9 0.5 all-gather.17.cloned.1.call-update
  193.4 0.0 all-gather.13.cloned.1.call-start
  193.5 71.5 %all-to-all-done = bf16[32,384,128]{2,1,0:T(8,128)(2,1)S(1)} async-done(((bf16[32,384,128]{2,1,0:T(8,128)(2,1)}), bf16[32,384,128]{2,1,0:T(8,128)(2,1)S(1)}, u32[]{:S(2)}, u32[]{:S(2)}) %all-to-all-start) | async-done | bytes 3145760 | tf_op jit(solution)/shard_map/all_to_all | solution.py:26
  264.9 0.4 convert_reduce_fusion.1
  265.4 0.0 copy-done
  265.4 0.2 fusion.8
  265.6 0.1 broadcast_in_dim.4
  265.6 16.4 %all_to_all.22 = f32[32,1,768]{2,1,0:T(1,128)S(1)} all-to-all(f32[32,1,768]{2,1,0:T(1,128)S(1)} %broadcast_in_dim.4), channel_id=1, replica_groups=mesh['ra_0'=8,'ra_1'=4,'cb'=4,'dp'=2] {'ra_0','ra_1'}, dimensions={0} | all-to-all | bytes 196608 | tf_op jit(solution)/shard_map/all_to_all | solution.py:32
  282.0 0.1 reduce_sum.75
  282.1 0.0 copy-done.1
  282.1 0.0 copy-done.2
  282.1 0.2 add_convert_fusion.1
  282.3 12.7 %all_gather.28 = bf16[384,512]{1,0:T(8,128)(2,1)} all-gather(bf16[384,128]{1,0:T(8,128)(2,1)S(1)} %add_convert_fusion.1), channel_id=1, replica_groups=mesh['ra_0'=8,'ra_1'=4,'cb'=4,'dp'=2] {'ra_1'}, dimensions={1}, use_global_device_ids=true | all-gather | bytes 491520 | tf_op jit(solution)/shard_map/all_gather | solution.py:14
  295.0 0.0 all-gather.13.cloned.1.call-update
  295.0 0.0 all-gather.15.cloned.1.call-done
  295.0 0.0 all-gather.17.cloned.1.call-done
  295.1 40.6 %all-gather.13.cloned.1.call-done = bf16[384,4096]{1,0:T(8,128)(2,1)} async-done(((bf16[384,512]{1,0:T(8,128)(2,1)}), bf16[384,4096]{1,0:T(8,128)(2,1)}) %all-gather.13.cloned.1.call-update) | async-done | bytes 3145744 | tf_op jit(solution)/shard_map/all_gather | solution.py:14
  335.7 7.8 %fusion.1 = bf16[48,32,8,128]{3,2,1,0:T(8,128)(2,1)S(1)} fusion(bf16[512,4096]{1,0:T(8,128)(2,1)} %all-gather.17.cloned.1.call-done, bf16[384,4096]{1,0:T(8,128)(2,1)} %all-gather.13.cloned.1.call-done, bf16[4096,512]{1,0:T(8,128)(2,1)} %all-gather.15.cloned.1.call-done), kind=kOutput, calls=%fused_computation.7 | convolution fusion | flops 3223388160 | bytes 14680064 | tf_op jit(solution)/shard_map/dot_general | solution.py:57
  343.5 0.9 copy.28
  344.4 0.0 copy-start.3
  344.4 0.0 copy-start.4
  344.4 79.6 %all_to_all.23 = bf16[32,384,128]{2,1,0:T(8,128)(2,1)S(1)} all-to-all(bf16[32,384,128]{2,1,0:T(8,128)(2,1)S(1)} %bitcast.23), channel_id=1, replica_groups=mesh['ra_0'=8,'ra_1'=4,'cb'=4,'dp'=2] {'ra_0','ra_1'}, dimensions={0} | all-to-all | bytes 6291456 | tf_op jit(solution)/shard_map/all_to_all | solution.py:26
  424.1 0.4 convert_reduce_fusion
  424.5 0.2 fusion.9
  424.7 0.1 broadcast_in_dim.5
  424.8 15.6 %all_to_all.24 = f32[32,1,768]{2,1,0:T(1,128)S(1)} all-to-all(f32[32,1,768]{2,1,0:T(1,128)S(1)} %broadcast_in_dim.5), channel_id=1, replica_groups=mesh['ra_0'=8,'ra_1'=4,'cb'=4,'dp'=2] {'ra_0','ra_1'}, dimensions={0} | all-to-all | bytes 196608 | tf_op jit(solution)/shard_map/all_to_all | solution.py:32
  440.4 0.1 reduce_sum.79
  440.5 0.0 copy-done.3
  440.5 0.0 copy-done.4
  440.5 0.8 add_convert_fusion
  (4 shorter events, 0.0 us)
Async XLA Ops:
  6.5 62.3 %all-gather.7.cloned.1.call-start = ((), (), s32[]{:S(2)}) async-start(), calls=%async_computation.4 | async-start | bytes 3538944 | tf_op jit(solution)/shard_map/all_gather | solution.py:14
  20.4 99.0 %all-gather.11.cloned.1.call-start = ((), (), s32[]{:S(2)}) async-start(), calls=%async_computation.6 | async-start | bytes 5242880 | tf_op jit(solution)/shard_map/all_gather | solution.py:58
  21.2 151.2 %all-gather.9.cloned.1.call-start = ((), (), s32[]{:S(2)}) async-start(), calls=%async_computation.5 | async-start | bytes 5242880 | tf_op jit(solution)/shard_map/all_gather | solution.py:54
  21.9 273.1 %all-gather.15.cloned.1.call-start = ((), (), s32[]{:S(2)}) async-start(), calls=%async_computation.8 | async-start | bytes 5242880 | tf_op jit(solution)/shard_map/all_gather | solution.py:54
  182.8 82.5 %copy-start = (bf16[384,128]{1,0:T(8,128)(2,1)S(1)}, bf16[384,128]{1,0:T(8,128)(2,1)}, u32[]{:S(2)}) copy-start(bf16[384,128]{1,0:T(8,128)(2,1)} %param.9) | copy-start | bytes 294916
  182.8 99.3 %copy-start.1 = (f32[128]{0:T(128)S(1)}, f32[128]{0:T(128)}, u32[]{:S(2)}) copy-start(f32[128]{0:T(128)} %param.15) | copy-start | bytes 1540
  182.8 99.3 %copy-start.2 = (f32[128]{0:T(128)S(1)}, f32[128]{0:T(128)}, u32[]{:S(2)}) copy-start(f32[128]{0:T(128)} %param.14) | copy-start | bytes 1540
  182.8 82.1 %all-to-all-start = ((bf16[32,384,128]{2,1,0:T(8,128)(2,1)}), bf16[32,384,128]{2,1,0:T(8,128)(2,1)S(1)}, u32[]{:S(2)}, u32[]{:S(2)}) async-start(bf16[32,384,128]{2,1,0:T(8,128)(2,1)} %bitcast.22), calls=%async_computation | async-start | bytes 6291456 | tf_op jit(solution)/shard_map/all_to_all | solution.py:26
  192.8 102.2 %all-gather.17.cloned.1.call-start = ((), (), s32[]{:S(2)}) async-start(), calls=%async_computation.9 | async-start | bytes 5242880 | tf_op jit(solution)/shard_map/all_gather | solution.py:58
  193.4 142.3 %all-gather.13.cloned.1.call-start = ((), (), s32[]{:S(2)}) async-start(), calls=%async_computation.7 | async-start | bytes 3538944 | tf_op jit(solution)/shard_map/all_gather | solution.py:14
  344.4 96.0 %copy-start.3 = (f32[128]{0:T(128)S(1)}, f32[128]{0:T(128)}, u32[]{:S(2)}) copy-start(f32[128]{0:T(128)} %param.17) | copy-start | bytes 1540
  344.4 96.0 %copy-start.4 = (f32[128]{0:T(128)S(1)}, f32[128]{0:T(128)}, u32[]{:S(2)}) copy-start(f32[128]{0:T(128)} %param.16) | copy-start | bytes 1540
Sparse Core Ops, SparseCore 0:
  20.5 48.2 all-gather.6
  70.7 48.7 all-gather.10
  121.2 51.0 all-gather.8
  174.0 51.0 all-gather.14
  226.8 51.0 all-gather.16
  295.1 40.5 all-gather.12
where the time goes:
time: 448 us
  waiting for transfers between devices  265 us (59%)
  blocking collectives  138 us (31%)
  matrix products  15.7 us (4%)
  between operations  13.6 us (3%)
  starting transfers between devices  10.2 us (2%)
    all_gather x2, waiting for transfers between devices, whole_of(): shard = lax.all_gather(shard, axis, axis=dim, tiled=True)  87 us
    all_to_all x1, blocking collectives, summed_on_arrival(): lax.all_to_all(cut_along(shard, dim, length), axis, 0, 0, tiled=True)  79.6 us
    all_to_all x1, waiting for transfers between devices, summed_on_arrival(): lax.all_to_all(cut_along(shard, dim, length), axis, 0, 0, tiled=True)  71.5 us
    all_gather x2, waiting for transfers between devices, sublayer(): lax.all_gather(up, 'cb', axis=0, tiled=True)  53 us
    all_gather x2, waiting for transfers between devices, sublayer(): lax.all_gather(down, 'cb', axis=1, tiled=True)  50.6 us
    all_to_all x2, blocking collectives, copy_for_each(): lax.all_to_all(jnp.broadcast_to(shard[None], (length, *shard.shape)), axi...  31.9 us
    all_gather x2, blocking collectives, whole_of(): shard = lax.all_gather(shard, axis, axis=dim, tiled=True)  26.5 us
    dot_general x2, matrix products, sublayer(): jnp.dot(hidden, lax.all_gather(down, 'cb', axis=1, tiled=True), preferred...  15.7 us
  transfers between devices with their start and end apart: 7, of which 5 were waited for; matrix products, arithmetic and copies ran while one was open for 3% of the time, Pallas kernels for 0%

commit v1 on v0

--- a/solution.py
+++ b/solution.py
@@ -7,6 +7,13 @@
 RA = ("ra_0", "ra_1")
 RESID = 1.4142135
 EPS = 0.5
+
+
+def masks_enter(content):
+    ndev = lax.axis_size("cb")
+    seen_now = tuple((ndev if num == 1 else 1 for num in range(content.ndim)))
+    then = jnp.tile(content, seen_now)
+    return lax.all_to_all(then, "cb", split_axis=1, concat_axis=1, tiled=True)
 
 
 def whole_of(shard, axes, dim):
@@ -54,9 +61,7 @@
         whole, lax.all_gather(up, "cb", axis=0, tiled=True), preferred_element_type=jnp.float32
     )
     hidden = jnp.square(jax.nn.relu(pre)).astype(jnp.bfloat16)
-    partial_sums = jnp.dot(
-        hidden, lax.all_gather(down, "cb", axis=1, tiled=True), preferred_element_type=jnp.float32
-    )
+    partial_sums = jnp.dot(hidden, masks_enter(down), preferred_element_type=jnp.float32)
     branch = summed_on_arrival(partial_sums.astype(jnp.bfloat16), RA, 1)
     mixed = RESID * x.astype(jnp.float32) + branch
     width = mixed.shape[1] * lax.axis_size(RA)

time: 448 us -> 406 us (0.906)
  waiting for transfers between devices: 265 us -> 112 us
  blocking collectives: 138 us -> 232 us
  local copies, waits for them, and re-layouts: 3.6 us -> 19.4 us
    all_to_all x0 -> x2, blocking collectives: none -> 98.2 us  [masks_enter(): return lax.all_to_all(then, 'cb', split_axis=1, concat_axis=1, tiled=True)]
    all_gather x2, waiting for transfers between devices: 87 us -> 0.01 us  [whole_of(): shard = lax.all_gather(shard, axis, axis=dim, tiled=True)]
    all_gather x2 -> x0, waiting for transfers between devices: 50.6 us -> none  [sublayer(): lax.all_gather(down, 'cb', axis=1, tiled=True)]
    all_gather x2, waiting for transfers between devices: 53 us -> 39.7 us  [sublayer(): lax.all_gather(up, 'cb', axis=0, tiled=True)]
    all_to_all x0 -> x2, local copies, waits for them, and re-layouts: none -> 12.4 us  [masks_enter(): return lax.all_to_all(then, 'cb', split_axis=1, concat_axis=1, tiled=True)]
    all_to_all x1, blocking collectives: 79.6 us -> 74.9 us  [summed_on_arrival(): lax.all_to_all(cut_along(shard, dim, length), axis, 0, 0, tiled=True)]
  transfers between devices with their start and end apart: 7 -> 5, of which waited for: 5 -> 2; matrix products, arithmetic and copies ran while one was open for 3% -> 4% of each run, Pallas kernels for 0% -> 0%
where the time goes in v1:
time: 406 us; the launch traced here: 405 us
  blocking collectives  232 us (57%)
  waiting for transfers between devices  112 us (28%)
  local copies, waits for them, and re-layouts  19.4 us (5%)
  matrix products  15.6 us (4%)
  between operations  13.3 us (3%)
  starting transfers between devices  10.1 us (2%)
    all_to_all x2, blocking collectives, masks_enter(): return lax.all_to_all(then, 'cb', split_axis=1, concat_axis=1, tiled=True)  98.2 us
    all_to_all x1, blocking collectives, summed_on_arrival(): lax.all_to_all(cut_along(shard, dim, length), axis, 0, 0, tiled=True)  74.9 us
    all_to_all x1, waiting for transfers between devices, summed_on_arrival(): lax.all_to_all(cut_along(shard, dim, length), axis, 0, 0, tiled=True)  71.3 us
    all_gather x2, waiting for transfers between devices, sublayer(): lax.all_gather(up, 'cb', axis=0, tiled=True)  39.7 us
    all_to_all x2, blocking collectives, copy_for_each(): lax.all_to_all(jnp.broadcast_to(shard[None], (length, *shard.shape)), axi...  31.9 us
    all_gather x2, blocking collectives, whole_of(): shard = lax.all_gather(shard, axis, axis=dim, tiled=True)  26.5 us
    dot_general x2, matrix products, sublayer(): jnp.dot(hidden, masks_enter(down), preferred_element_type=jnp.float32)  15.6 us
    all_to_all x2, local copies, waits for them, and re-layouts, masks_enter(): return lax.all_to_all(then, 'cb', split_axis=1, concat_axis=1, tiled=True)  12.4 us
  transfers between devices with their start and end apart: 5, of which 2 were waited for; matrix products, arithmetic and copies ran while one was open for 4% of the time, Pallas kernels for 0%

profile of v1, /device:TPU:2, one launch (start us, length us, event | category | flops | bytes accessed | tf_op | source)
XLA Modules:
  0.0 404.8 jit_solution(9513310780894151448)
XLA Ops:
  6.5 0.0 all-gather.5.cloned.1.call-start
  6.5 13.8 %all_gather.18 = bf16[384,512]{1,0:T(8,128)(2,1)} all-gather(bf16[384,128]{1,0:T(8,128)(2,1)} %param.9), channel_id=1, replica_groups=mesh['ra_0'=8,'ra_1'=4,'cb'=4,'dp'=2] {'ra_1'}, dimensions={1}, use_global_device_ids=true | all-gather | bytes 491520 | tf_op jit(solution)/shard_map/all_gather | solution.py:21
  20.4 0.0 all-gather.5.cloned.1.call-update
  20.4 0.0 all-gather.7.cloned.1.call-start
  20.4 0.7 all-gather.7.cloned.1.call-update
  21.1 1.7 tile.4
  22.9 50.6 %all_to_all.40 = bf16[512,4,1024]{2,0,1:T(8,128)(2,1)} all-to-all(bf16[512,4,1024]{2,0,1:T(8,128)(2,1)S(1)} %tile.4), channel_id=1, replica_groups=mesh['ra_0'=8,'ra_1'=4,'cb'=4,'dp'=2] {'cb'}, dimensions={1} | all-to-all | bytes 8388608 | tf_op jit(solution)/shard_map/all_to_all | solution.py:16
  73.5 6.2 %copy.20 = bf16[512,4,1024]{0,2,1:T(8,128)(2,1)} copy(bf16[512,4,1024]{2,0,1:T(8,128)(2,1)} %all_to_all.40) | data formatting | bytes 8388608 | tf_op jit(solution)/shard_map/all_to_all | solution.py:16
  79.7 0.0 all-gather.5.cloned.1.call-done
  79.7 39.7 %all-gather.7.cloned.1.call-done = bf16[4096,512]{1,0:T(8,128)(2,1)} async-done(((bf16[1024,512]{1,0:T(8,128)(2,1)}), bf16[4096,512]{1,0:T(8,128)(2,1)}) %all-gather.7.cloned.1.call-update) | async-done | bytes 4194320 | tf_op jit(solution)/shard_map/all_gather | solution.py:61
  119.4 7.8 %fusion = bf16[48,32,8,128]{3,2,1,0:T(8,128)(2,1)S(1)} fusion(bf16[512,4096]{0,1:T(8,128)(2,1)} %bitcast.26, bf16[384,4096]{1,0:T(8,128)(2,1)} %all-gather.5.cloned.1.call-done, bf16[4096,512]{1,0:T(8,128)(2,1)} %all-gather.7.cloned.1.call-done), kind=kOutput, calls=%fused_computation.6 | convolution fusion | flops 3223388160 | bytes 14680064 | tf_op jit(solution)/shard_map/dot_general | solution.py:64
  127.2 2.6 copy.37
  129.8 0.0 copy-start
  129.8 0.0 copy-start.1
  129.8 0.0 copy-start.2
  129.8 10.0 %all-to-all-start.1 = ((bf16[32,384,128]{2,1,0:T(8,128)(2,1)}), bf16[32,384,128]{2,1,0:T(8,128)(2,1)S(1)}, u32[]{:S(2)}, u32[]{:S(2)}) async-start(bf16[32,384,128]{2,1,0:T(8,128)(2,1)} %bitcast.24), calls=%async_computation.1 | async-start | bytes 6291456 | tf_op jit(solution)/shard_map/all_to_all | solution.py:33
  139.8 0.0 all-gather.11.cloned.1.call-start
  139.8 0.7 all-gather.11.cloned.1.call-update
  140.5 0.0 all-gather.9.cloned.1.call-start
  140.6 71.3 %all-to-all-done.1 = bf16[32,384,128]{2,1,0:T(8,128)(2,1)S(1)} async-done(((bf16[32,384,128]{2,1,0:T(8,128)(2,1)}), bf16[32,384,128]{2,1,0:T(8,128)(2,1)S(1)}, u32[]{:S(2)}, u32[]{:S(2)}) %all-to-all-start.1) | async-done | bytes 3145760 | tf_op jit(solution)/shard_map/all_to_all | solution.py:33
  211.9 0.4 convert_reduce_fusion.1
  212.3 0.0 copy-done
  212.3 0.2 fusion.8
  212.5 0.1 broadcast_in_dim.4
  212.6 16.4 %all_to_all.41 = f32[32,1,768]{2,1,0:T(1,128)S(1)} all-to-all(f32[32,1,768]{2,1,0:T(1,128)S(1)} %broadcast_in_dim.4), channel_id=1, replica_groups=mesh['ra_0'=8,'ra_1'=4,'cb'=4,'dp'=2] {'ra_0','ra_1'}, dimensions={0} | all-to-all | bytes 196608 | tf_op jit(solution)/shard_map/all_to_all | solution.py:39
  228.9 0.1 reduce_sum.75
  229.0 0.0 copy-done.1
  229.0 0.0 copy-done.2
  229.1 0.2 add_convert_fusion.1
  229.2 12.7 %all_gather.21 = bf16[384,512]{1,0:T(8,128)(2,1)} all-gather(bf16[384,128]{1,0:T(8,128)(2,1)S(1)} %add_convert_fusion.1), channel_id=1, replica_groups=mesh['ra_0'=8,'ra_1'=4,'cb'=4,'dp'=2] {'ra_1'}, dimensions={1}, use_global_device_ids=true | all-gather | bytes 491520 | tf_op jit(solution)/shard_map/all_gather | solution.py:21
  241.9 0.0 all-gather.9.cloned.1.call-update
  241.9 1.7 tile.5
  243.7 47.6 %all_to_all.42 = bf16[512,4,1024]{2,0,1:T(8,128)(2,1)} all-to-all(bf16[512,4,1024]{2,0,1:T(8,128)(2,1)S(1)} %tile.5), channel_id=1, replica_groups=mesh['ra_0'=8,'ra_1'=4,'cb'=4,'dp'=2] {'cb'}, dimensions={1} | all-to-all | bytes 8388608 | tf_op jit(solution)/shard_map/all_to_all | solution.py:16
  291.3 6.2 %copy.23 = bf16[512,4,1024]{0,2,1:T(8,128)(2,1)} copy(bf16[512,4,1024]{2,0,1:T(8,128)(2,1)} %all_to_all.42) | data formatting | bytes 8388608 | tf_op jit(solution)/shard_map/all_to_all | solution.py:16
  297.5 0.0 all-gather.11.cloned.1.call-done
  297.5 0.0 all-gather.9.cloned.1.call-done
  297.5 7.8 %fusion.1 = bf16[48,32,8,128]{3,2,1,0:T(8,128)(2,1)S(1)} fusion(bf16[512,4096]{0,1:T(8,128)(2,1)} %bitcast.27, bf16[384,4096]{1,0:T(8,128)(2,1)} %all-gather.9.cloned.1.call-done, bf16[4096,512]{1,0:T(8,128)(2,1)} %all-gather.11.cloned.1.call-done), kind=kOutput, calls=%fused_computation.7 | convolution fusion | flops 3223388160 | bytes 14680064 | tf_op jit(solution)/shard_map/dot_general | solution.py:64
  305.3 0.9 copy.36
  306.2 0.0 copy-start.3
  306.2 0.0 copy-start.4
  306.2 74.9 %all_to_all.43 = bf16[32,384,128]{2,1,0:T(8,128)(2,1)S(1)} all-to-all(bf16[32,384,128]{2,1,0:T(8,128)(2,1)S(1)} %bitcast.25), channel_id=1, replica_groups=mesh['ra_0'=8,'ra_1'=4,'cb'=4,'dp'=2] {'ra_0','ra_1'}, dimensions={0} | all-to-all | bytes 6291456 | tf_op jit(solution)/shard_map/all_to_all | solution.py:33
  381.2 0.4 convert_reduce_fusion
  381.6 0.2 fusion.9
  381.8 0.1 broadcast_in_dim.5
  381.8 15.5 %all_to_all.44 = f32[32,1,768]{2,1,0:T(1,128)S(1)} all-to-all(f32[32,1,768]{2,1,0:T(1,128)S(1)} %broadcast_in_dim.5), channel_id=1, replica_groups=mesh['ra_0'=8,'ra_1'=4,'cb'=4,'dp'=2] {'ra_0','ra_1'}, dimensions={0} | all-to-all | bytes 196608 | tf_op jit(solution)/shard_map/all_to_all | solution.py:39
  397.4 0.1 reduce_sum.79
  397.5 0.0 copy-done.3
  397.5 0.0 copy-done.4
  397.5 0.8 add_convert_fusion
  (4 shorter events, 0.0 us)
Async XLA Ops:
  6.5 73.2 %all-gather.5.cloned.1.call-start = ((), (), s32[]{:S(2)}) async-start(), calls=%async_computation.6 | async-start | bytes 3538944 | tf_op jit(solution)/shard_map/all_gather | solution.py:21
  20.4 99.0 %all-gather.7.cloned.1.call-start = ((), (), s32[]{:S(2)}) async-start(), calls=%async_computation.7 | async-start | bytes 5242880 | tf_op jit(solution)/shard_map/all_gather | solution.py:61
  129.8 82.5 %copy-start = (bf16[384,128]{1,0:T(8,128)(2,1)S(1)}, bf16[384,128]{1,0:T(8,128)(2,1)}, u32[]{:S(2)}) copy-start(bf16[384,128]{1,0:T(8,128)(2,1)} %param.9) | copy-start | bytes 294916
  129.8 99.3 %copy-start.1 = (f32[128]{0:T(128)S(1)}, f32[128]{0:T(128)}, u32[]{:S(2)}) copy-start(f32[128]{0:T(128)} %param.15) | copy-start | bytes 1540
  129.8 99.3 %copy-start.2 = (f32[128]{0:T(128)S(1)}, f32[128]{0:T(128)}, u32[]{:S(2)}) copy-start(f32[128]{0:T(128)} %param.14) | copy-start | bytes 1540
  129.8 82.1 %all-to-all-start.1 = ((bf16[32,384,128]{2,1,0:T(8,128)(2,1)}), bf16[32,384,128]{2,1,0:T(8,128)(2,1)S(1)}, u32[]{:S(2)}, u32[]{:S(2)}) async-start(bf16[32,384,128]{2,1,0:T(8,128)(2,1)} %bitcast.24), calls=%async_computation.1 | async-start | bytes 6291456 | tf_op jit(solution)/shard_map/all_to_all | solution.py:33
  139.8 157.7 %all-gather.11.cloned.1.call-start = ((), (), s32[]{:S(2)}) async-start(), calls=%async_computation.9 | async-start | bytes 5242880 | tf_op jit(solution)/shard_map/all_gather | solution.py:61
  140.5 157.0 %all-gather.9.cloned.1.call-start = ((), (), s32[]{:S(2)}) async-start(), calls=%async_computation.8 | async-start | bytes 3538944 | tf_op jit(solution)/shard_map/all_gather | solution.py:21
  306.2 91.3 %copy-start.3 = (f32[128]{0:T(128)S(1)}, f32[128]{0:T(128)}, u32[]{:S(2)}) copy-start(f32[128]{0:T(128)} %param.17) | copy-start | bytes 1540
  306.2 91.3 %copy-start.4 = (f32[128]{0:T(128)S(1)}, f32[128]{0:T(128)}, u32[]{:S(2)}) copy-start(f32[128]{0:T(128)} %param.16) | copy-start | bytes 1540
Sparse Core Ops, SparseCore 0:
  20.5 48.2 all-gather.4
  70.6 48.7 all-gather.6
  142.4 51.0 all-gather.10
  242.1 40.5 all-gather.8
